TPU v7x, 32 devices: a whole 2x2x4 slice. The times are simulated.
32 devices in a mesh: ep: 8 (over z, y), tp: 4 (over x, core).
Axes of the slice: x: 2, y: 2, z: 4, core: 2. Of those that a mesh axis runs over, the one named last changes fastest.
Arguments:
- tokens: bfloat16 [128, 2048], P('ep'), may hold values from -6 to 6
- norm_gain: bfloat16 [2048], replicated, may hold values from 0.099609375 to 1.8984375
- query_weight: bfloat16 [2048, 1024], P('ep', 'tp'), may hold values from -0.125 to 0.125
- key_weight: bfloat16 [2048, 1024], P('ep', 'tp'), may hold values from -0.125 to 0.125
- value_weight: bfloat16 [2048, 2048], P('ep', 'tp'), may hold values from -0.125 to 0.125
- outgate_weight: bfloat16 [2048, 2048], P('ep', 'tp'), may hold values from -0.125 to 0.125
- beta_weight: bfloat16 [2048, 16], replicated, may hold values from -0.125 to 0.125
- decay_weight: bfloat16 [2048, 16], replicated, may hold values from -0.125 to 0.125
- decay_rate: float32 [16], P('tp'), may hold values from 0.02 to 6
- decay_bias: float32 [16], P('tp'), may hold values from -3 to 3
- head_gain: bfloat16 [128], replicated, may hold values from 0.099609375 to 1.8984375
- recurrent: float32 [128, 16, 128, 128], P('ep', 'tp'), may hold values from -3 to 3
- output_weight: bfloat16 [2048, 2048], P('tp', 'ep'), may hold values from -0.125 to 0.125
- ffn_gain: bfloat16 [2048], replicated, may hold values from 0.099609375 to 1.8984375
- routes: int32 [128, 4], P('ep'), may hold values from 0 to 7, all different within a row; in each aligned block of 16 rows (0 to 15, 16 to 31, ...) at most 16 rows name the same one
- route_weight: float32 [128, 4], P('ep'), may hold values from 0.1 to 1
- expert_gate: bfloat16 [8, 2048, 512], P('ep', None, 'tp'), may hold values from -0.125 to 0.125
- expert_up: bfloat16 [8, 2048, 512], P('ep', None, 'tp'), may hold values from -0.125 to 0.125
- expert_down: bfloat16 [8, 512, 2048], P('ep', 'tp'), may hold values from -0.25 to 0.25
- shared_gate: bfloat16 [2048, 512], P('ep', 'tp'), may hold values from -0.125 to 0.125
- shared_up: bfloat16 [2048, 512], P('ep', 'tp'), may hold values from -0.125 to 0.125
- shared_down: bfloat16 [512, 2048], P('tp', 'ep'), may hold values from -0.25 to 0.25
- branch_gate: bfloat16 [2048], replicated, may hold values from -0.125 to 0.125
Outputs:
- layer_out: bfloat16 [128, 2048], P('ep')
- new_state: float32 [128, 16, 128, 128], P('ep', 'tp')
Inputs may be any that keep to these rules, and one draw needn't show every extreme that they name: `routes`: each row names 4 different experts. Among the rows of one aligned block of 16 rows no expert is named more than 16 times, and some block reaches it: one expert is named exactly 16 times there.
All inputs are finite; a program needn't handle non-finite values.
Results may differ from a plain program's by a relative error of at most 0.019.
Values may be sent and summed in bfloat16 or wider, within the bound.
A program may use at most 64 MiB of HBM per device.

v0:
```python
import jax
import jax.numpy as jnp
from jax import lax
from jax.sharding import PartitionSpec as P

EPS = 1e-06
ROUTED_SCALE = 2.5


def rms_scale(values, gain):
    values = values.astype(jnp.float32)
    return (
        values
        * lax.rsqrt(jnp.mean(values * values, axis=-1, keepdims=True) + EPS)
        * gain.astype(jnp.float32)
    )


def unit_rows(values):
    return values * lax.rsqrt(jnp.sum(values * values, axis=-1, keepdims=True) + EPS)


def per_device(
    tokens,
    norm_gain,
    query_weight,
    key_weight,
    value_weight,
    outgate_weight,
    beta_weight,
    decay_weight,
    decay_rate,
    decay_bias,
    head_gain,
    recurrent,
    output_weight,
    ffn_gain,
    routes,
    route_weight,
    expert_gate,
    expert_up,
    expert_down,
    shared_gate,
    shared_up,
    shared_down,
    branch_gate,
):
    ep_count = lax.axis_size("ep")
    seq_local, width = tokens.shape
    heads_local, key_dim, value_dim = (recurrent.shape[1], recurrent.shape[2], recurrent.shape[3])
    normed = rms_scale(tokens, norm_gain).astype(jnp.bfloat16)
    query_cols = query_weight.shape[1]
    value_cols = value_weight.shape[1]
    spread = lax.all_to_all(normed, "ep", split_axis=1, concat_axis=0, tiled=True)
    stacked = jnp.concatenate((query_weight, key_weight, value_weight, outgate_weight), axis=1)
    token_block = spread
    projected = lax.psum_scatter(
        jnp.dot(token_block, stacked, preferred_element_type=jnp.float32),
        "ep",
        scatter_dimension=0,
        tiled=True,
    )
    query_sum = projected[:, :query_cols]
    key_sum = projected[:, query_cols : 2 * query_cols]
    value_sum = projected[:, 2 * query_cols : 2 * query_cols + value_cols]
    gate_sum = projected[:, 2 * query_cols + value_cols :]
    query_proj = query_sum.astype(jnp.bfloat16)
    key_proj = key_sum.astype(jnp.bfloat16)
    value_proj = value_sum.astype(jnp.bfloat16)
    gate_proj = gate_sum.astype(jnp.bfloat16)
    key_local = query_cols // key_dim
    repeat_count = heads_local // key_local
    queries = unit_rows(
        jax.nn.silu(query_proj.astype(jnp.float32)).reshape(seq_local, key_local, key_dim)
    )
    queries = jnp.repeat(queries, repeat_count, axis=1) * key_dim ** (-0.5)
    key_rows = unit_rows(
        jax.nn.silu(key_proj.astype(jnp.float32)).reshape(seq_local, key_local, key_dim)
    )
    key_rows = jnp.repeat(key_rows, repeat_count, axis=1)
    value_rows = jax.nn.silu(value_proj.astype(jnp.float32)).reshape(
        seq_local, heads_local, value_dim
    )
    head_start = lax.axis_index("tp") * heads_local
    beta_logit = jnp.dot(
        normed,
        lax.dynamic_slice_in_dim(beta_weight, head_start, heads_local, 1),
        preferred_element_type=jnp.float32,
    )
    decay_logit = jnp.dot(
        normed,
        lax.dynamic_slice_in_dim(decay_weight, head_start, heads_local, 1),
        preferred_element_type=jnp.float32,
    )
    strength = jax.nn.sigmoid(beta_logit)
    retain = jnp.exp(-decay_rate[None, :] * jax.nn.softplus(decay_logit + decay_bias[None, :]))
    decayed = recurrent * retain[:, :, None, None]
    predicted = jnp.einsum("shde,shd->she", decayed, key_rows, precision=lax.Precision.HIGHEST)
    correction = strength[:, :, None] * (value_rows - predicted)
    new_state = decayed + key_rows[:, :, :, None] * correction[:, :, None, :]
    readout = jnp.einsum("shde,shd->she", new_state, queries, precision=lax.Precision.HIGHEST)
    out_gate = jax.nn.silu(gate_proj.astype(jnp.float32)).reshape(seq_local, heads_local, value_dim)
    heads_out = (
        (rms_scale(readout, head_gain) * out_gate)
        .astype(jnp.bfloat16)
        .reshape(seq_local, heads_local * value_dim)
    )
    partial_mix = jnp.dot(
        heads_out,
        lax.all_gather(output_weight, "ep", axis=1, tiled=True),
        preferred_element_type=jnp.float32,
    )
    partial_mix = partial_mix.astype(jnp.bfloat16).astype(jnp.float32)
    mixed = lax.psum(partial_mix.astype(jnp.bfloat16), "tp").astype(jnp.float32)
    residual = (tokens.astype(jnp.float32) + mixed).astype(jnp.bfloat16)
    ffn_in = rms_scale(residual, ffn_gain).astype(jnp.bfloat16)
    token_block = ffn_in
    shared_g = jnp.dot(
        token_block,
        lax.all_gather(shared_gate, "ep", axis=0, tiled=True),
        preferred_element_type=jnp.float32,
    )
    shared_u = jnp.dot(
        token_block,
        lax.all_gather(shared_up, "ep", axis=0, tiled=True),
        preferred_element_type=jnp.float32,
    )
    shared_act = (jax.nn.silu(shared_g) * shared_u).astype(jnp.bfloat16)
    shared_partial = jnp.dot(
        shared_act,
        lax.all_gather(shared_down, "ep", axis=1, tiled=True),
        preferred_element_type=jnp.float32,
    )
    shared_out = lax.psum(
        shared_partial.astype(jnp.bfloat16).astype(jnp.float32).astype(jnp.bfloat16), "tp"
    ).astype(jnp.float32)
    topk = routes.shape[1]
    pair_count = seq_local * topk
    capacity = 2 * ((pair_count + ep_count - 1) // ep_count)
    expert_ids = routes.reshape(pair_count)
    onehot = (expert_ids[:, None] == jnp.arange(ep_count)[None, :]).astype(jnp.float32)
    earlier = (jnp.arange(pair_count)[:, None] > jnp.arange(pair_count)[None, :]).astype(
        jnp.float32
    )
    slots = jnp.sum(
        jnp.dot(earlier, onehot, precision=lax.Precision.HIGHEST) * onehot, axis=1
    ).astype(jnp.int32)
    target = expert_ids * capacity + slots
    placement_matrix = (target[:, None] == jnp.arange(ep_count * capacity)[None, :]).astype(
        jnp.bfloat16
    )
    dispatch_matrix = jnp.sum(
        placement_matrix.reshape(seq_local, topk, ep_count * capacity).astype(jnp.float32), axis=1
    ).astype(jnp.bfloat16)
    outgoing = jnp.dot(dispatch_matrix.T, ffn_in, preferred_element_type=jnp.float32).astype(
        jnp.bfloat16
    )
    outgoing = outgoing.reshape(ep_count, capacity, width)
    received = lax.all_to_all(outgoing, "ep", split_axis=0, concat_axis=0, tiled=True)
    flat_rows = received.reshape(-1, width)
    gate_part = jnp.dot(flat_rows, expert_gate[0], preferred_element_type=jnp.float32)
    up_part = jnp.dot(flat_rows, expert_up[0], preferred_element_type=jnp.float32)
    act = (jax.nn.silu(gate_part) * up_part).astype(jnp.bfloat16)
    partial_rows = (
        jnp.dot(act, expert_down[0], preferred_element_type=jnp.float32)
        .astype(jnp.bfloat16)
        .astype(jnp.float32)
    )
    summed = lax.psum(partial_rows.astype(jnp.bfloat16), "tp")
    returned = lax.all_to_all(
        summed.reshape(received.shape), "ep", split_axis=0, concat_axis=0, tiled=True
    )
    scaled = route_weight / jnp.sum(route_weight, axis=1, keepdims=True) * ROUTED_SCALE
    branch = jax.nn.sigmoid(jnp.dot(ffn_in, branch_gate, preferred_element_type=jnp.float32))
    pair_out = jnp.dot(
        placement_matrix,
        returned.reshape(ep_count * capacity, width),
        preferred_element_type=jnp.float32,
    )
    moe = jnp.sum(pair_out.reshape(seq_local, topk, width) * scaled[:, :, None], axis=1)
    layer_out = (residual.astype(jnp.float32) + moe + branch[:, None] * shared_out).astype(
        jnp.bfloat16
    )
    return (layer_out, new_state)


def solution(mesh):
    return jax.shard_map(
        per_device,
        mesh=mesh,
        in_specs=(
            P("ep", None),
            P(),
            P("ep", "tp"),
            P("ep", "tp"),
            P("ep", "tp"),
            P("ep", "tp"),
            P(),
            P(),
            P("tp"),
            P("tp"),
            P(),
            P("ep", "tp", None, None),
            P("tp", "ep"),
            P(),
            P("ep", None),
            P("ep", None),
            P("ep", None, "tp"),
            P("ep", None, "tp"),
            P("ep", "tp", None),
            P("ep", "tp"),
            P("ep", "tp"),
            P("tp", "ep"),
            P(),
        ),
        out_specs=(P("ep", None), P("ep", "tp", None, None)),
        check_vma=False,
    )
```

profile of v0, /device:TPU:0, one launch (start us, length us, event | category | flops | bytes accessed | tf_op | source)
XLA Modules:
  0.0 310.8 jit_solution(1554573020818032295)
XLA Ops:
  7.3 0.7 convert_element_type.97
  8.0 1.0 fusion.27
  9.0 0.9 fusion.29
  9.9 14.0 %all_to_all.29 = bf16[16,8,256]{2,0,1:T(8,128)(2,1)S(1)} all-to-all(bf16[16,8,256]{2,0,1:T(8,128)(2,1)S(1)} %bitcast.82), channel_id=1, replica_groups=mesh['ep'=8,'tp'=4] {'ep'}, dimensions={1} | all-to-all | bytes 131072 | tf_op jit(solution)/shard_map/all_to_all | solution.py:54
  24.0 2.3 fusion.14
  26.3 0.7 all-gather.2.cloned.1.call-update
  27.1 0.9 fusion.70
  28.1 0.9 fusion.9
  29.1 31.9 %all_gather.13 = bf16[2048,128]{1,0:T(8,128)(2,1)S(1)} all-gather(bf16[256,128]{1,0:T(8,128)(2,1)S(1)} %copy-done.6), channel_id=1, replica_groups=mesh['ep'=8,'tp'=4] {'ep'}, dimensions={0}, use_global_device_ids=true | all-gather | bytes 589824 | tf_op jit(solution)/shard_map/all_gather | solution.py:120
  61.5 25.8 %reduce-scatter.2.cloned.1.call-done = f32[16,1536]{1,0:T(8,128)} async-done(((f32[128,1536]{1,0:T(8,128)}), f32[16,1536]{1,0:T(8,128)}) %reduce-scatter.2.cloned.1.call-update) | async-done | bytes 98320 | tf_op jit(solution)/shard_map/reduce_scatter | solution.py:57
  87.3 0.9 convert.7
  88.8 5.8 %fusion = f32[16,4,1,128]{3,2,1,0:T(1,128)S(1)} fusion(f32[16,4,128,1]{2,3,1,0:T(1,128)S(1)} %bitcast.77, f32[16,4,128,128]{3,2,1,0:T(8,128)} %param.34, f32[16,4]{1,0:T(8,128)S(1)} %copy.43), kind=kOutput, calls=%fused_computation.1 | convolution fusion | flops 13631488 | bytes 4260096 | tf_op jit(solution)/shard_map/shde,shd->she/dot_general | solution.py:98
  94.7 1.5 multiply_add_fusion
  96.2 2.0 copy-done.2
  98.2 3.6 %fusion.79 = f32[16,4,1,128]{3,2,1,0:T(1,128)S(1)} fusion(f32[16,4,128,128]{3,2,1,0:T(8,128)S(1)} %multiply_add_fusion, f32[16,4,128,1]{2,3,1,0:T(1,128)S(1)} %bitcast.84), kind=kOutput, calls=%fused_computation.121 | convolution fusion | flops 12582912 | bytes 4259840 | tf_op jit(solution)/shard_map/shde,shd->she/dot_general | solution.py:101
  102.1 36.7 %all-gather.2.cloned.1.call-done = bf16[512,2048]{1,0:T(8,128)(2,1)} async-done(((bf16[512,256]{1,0:T(8,128)(2,1)}), bf16[512,2048]{1,0:T(8,128)(2,1)}) %all-gather.2.cloned.1.call-update) | async-done | bytes 2097168 | tf_op jit(solution)/shard_map/all_gather | solution.py:110
  138.7 2.6 convolution_convert_fusion.3
  141.5 29.9 %all-reduce.4.cloned.1.call-done = bf16[16,2048]{1,0:T(8,128)(2,1)} async-done(((bf16[16,2048]{1,0:T(8,128)(2,1)}), bf16[16,2048]{1,0:T(8,128)(2,1)}) %all-reduce.4.cloned.1.call-update) | async-done | bytes 65552 | tf_op jit(solution)/shard_map/psum | solution.py:114
  171.4 1.0 fusion.31
  172.4 0.9 fusion.33
  173.3 1.1 convolution_convert_fusion.1
  174.4 5.5 %all-to-all-start.1 = ((bf16[8,16,2048]{2,1,0:T(8,128)(2,1)}), bf16[8,16,2048]{2,1,0:T(8,128)(2,1)S(1)}, u32[]{:S(2)}, u32[]{:S(2)}) async-start(bf16[8,16,2048]{2,1,0:T(8,128)(2,1)} %bitcast.13), calls=%async_computation.2 | async-start | bytes 1048576 | tf_op jit(solution)/shard_map/all_to_all | solution.py:159
  180.0 37.8 %all_gather.14 = bf16[2048,128]{1,0:T(8,128)(2,1)S(1)} all-gather(bf16[256,128]{1,0:T(8,128)(2,1)S(1)} %copy-done.7), channel_id=1, replica_groups=mesh['ep'=8,'tp'=4] {'ep'}, dimensions={0}, use_global_device_ids=true | all-gather | bytes 589824 | tf_op jit(solution)/shard_map/all_gather | solution.py:125
  217.8 31.3 %all_gather.15 = bf16[128,2048]{1,0:T(8,128)(2,1)S(1)} all-gather(bf16[128,256]{1,0:T(8,128)(2,1)S(1)} %copy-done.8), channel_id=1, replica_groups=mesh['ep'=8,'tp'=4] {'ep'}, dimensions={1}, use_global_device_ids=true | all-gather | bytes 589824 | tf_op jit(solution)/shard_map/all_gather | solution.py:131
  249.3 1.0 convolution_convert_fusion.2
  250.3 0.3 fusion.25
  250.6 2.4 convolution_convert_fusion
  253.0 30.3 %all-reduce.6.cloned.1.call-done = (bf16[8,16,2048]{2,1,0:T(8,128)(2,1)}, bf16[16,2048]{1,0:T(8,128)(2,1)}) async-done(((bf16[8,16,2048]{2,1,0:T(8,128)(2,1)}, bf16[16,2048]{1,0:T(8,128)(2,1)}), (bf16[8,16,2048]{2,1,0:T(8,128)(2,1)}, bf16[16,2048]{1,0:T(8,128)(2,1)})) %all-reduce.6.cloned.1.call-update) | async-done | bytes 589840 | tf_op jit(solution)/shard_map/psum | solution.py:169
  283.3 5.5 %all-to-all-start.2 = ((bf16[8,16,2048]{2,1,0:T(8,128)(2,1)}), bf16[8,16,2048]{2,1,0:T(8,128)(2,1)S(1)}, u32[]{:S(2)}, u32[]{:S(2)}) async-start(bf16[8,16,2048]{2,1,0:T(8,128)(2,1)} %get-tuple-element.2), calls=%async_computation.3 | async-start | bytes 1048576 | tf_op jit(solution)/shard_map/all_to_all | solution.py:170
  289.0 13.4 %all-to-all-done.2 = bf16[8,16,2048]{2,1,0:T(8,128)(2,1)S(1)} async-done(((bf16[8,16,2048]{2,1,0:T(8,128)(2,1)}), bf16[8,16,2048]{2,1,0:T(8,128)(2,1)S(1)}, u32[]{:S(2)}, u32[]{:S(2)}) %all-to-all-start.2) | async-done | bytes 524320 | tf_op jit(solution)/shard_map/all_to_all | solution.py:170
  302.4 0.3 fusion.3
  302.7 1.6 fusion.35
  (78 shorter events, 2.2 us)
Async XLA Ops:
  7.2 243.4 %copy-start = (bf16[1,128,2048]{2,1,0:T(8,128)(2,1)S(1)}, bf16[1,128,2048]{2,1,0:T(8,128)(2,1)}, u32[]{:S(2)}) copy-start(bf16[1,128,2048]{2,1,0:T(8,128)(2,1)} %param.41) | copy-start | bytes 1572868
  7.2 19.9 %copy-start.13 = (f32[4]{0:T(128)S(1)}, f32[4]{0:T(128)}, u32[]{:S(2)}) copy-start(f32[4]{0:T(128)} %param.31) | copy-start | bytes 52
  7.2 19.9 %copy-start.14 = (f32[4]{0:T(128)S(1)}, f32[4]{0:T(128)}, u32[]{:S(2)}) copy-start(f32[4]{0:T(128)} %param.32) | copy-start | bytes 52
  7.2 21.9 %copy-start.15 = (bf16[128]{0:T(256)(128)(2,1)S(1)}, bf16[128]{0:T(256)(128)(2,1)}, u32[]{:S(2)}) copy-start(bf16[128]{0:T(256)(128)(2,1)} %param.33) | copy-start | bytes 772
  7.2 21.9 %copy-start.6 = (bf16[256,128]{1,0:T(8,128)(2,1)S(1)}, bf16[256,128]{1,0:T(8,128)(2,1)}, u32[]{:S(2)}) copy-start(bf16[256,128]{1,0:T(8,128)(2,1)} %param.42) | copy-start | bytes 196612
  7.2 53.8 %copy-start.9 = (s32[16,4]{0,1:T(4,128)S(1)}, s32[16,4]{0,1:T(4,128)}, u32[]{:S(2)}) copy-start(s32[16,4]{0,1:T(4,128)} %param.37) | copy-start | bytes 772
  7.2 80.1 %reduce-scatter.2.cloned.1.call-start = ((), (), s32[]{:S(2)}) async-start(), calls=%async_computation.4 | async-start | bytes 884736 | tf_op jit(solution)/shard_map/reduce_scatter | solution.py:57
  26.2 112.5 %all-gather.2.cloned.1.call-start = ((), (), s32[]{:S(2)}) async-start(), calls=%async_computation.5 | async-start | bytes 2359296 | tf_op jit(solution)/shard_map/all_gather | solution.py:110
  27.0 144.4 %all-reduce.4.cloned.1.call-start = ((), (), s32[]{:S(2)}) async-start(), calls=%async_computation.6 | async-start | bytes 131072 | tf_op jit(solution)/shard_map/psum | solution.py:114
  88.3 6.3 %copy-start.1 = (f32[16,4,128,128]{3,2,1,0:T(8,128)S(1)}, f32[16,4,128,128]{3,2,1,0:T(8,128)}, u32[]{:S(2)}) copy-start(f32[16,4,128,128]{3,2,1,0:T(8,128)} %param.34) | copy-start | bytes 12582916
  96.2 2.0 copy-start.2
  96.2 45.2 %copy-start.11 = (bf16[2048]{0:T(1024)(128)(2,1)S(1)}, bf16[2048]{0:T(1024)(128)(2,1)}, u32[]{:S(2)}) copy-start(bf16[2048]{0:T(1024)(128)(2,1)} %param.36) | copy-start | bytes 12292
  96.2 75.2 %copy-start.3 = (bf16[16,2048]{1,0:T(8,128)(2,1)S(1)}, bf16[16,2048]{1,0:T(8,128)(2,1)}, u32[]{:S(2)}) copy-start(bf16[16,2048]{1,0:T(8,128)(2,1)} %param.23) | copy-start | bytes 196612
  98.2 81.8 %copy-start.7 = (bf16[256,128]{1,0:T(8,128)(2,1)S(1)}, bf16[256,128]{1,0:T(8,128)(2,1)}, u32[]{:S(2)}) copy-start(bf16[256,128]{1,0:T(8,128)(2,1)} %param.43) | copy-start | bytes 196612
  98.2 119.6 %copy-start.8 = (bf16[128,256]{1,0:T(8,128)(2,1)S(1)}, bf16[128,256]{1,0:T(8,128)(2,1)}, u32[]{:S(2)}) copy-start(bf16[128,256]{1,0:T(8,128)(2,1)} %param.44) | copy-start | bytes 196612
  101.9 148.4 %copy-start.5 = (bf16[1,2048,128]{2,1,0:T(8,128)(2,1)S(1)}, bf16[1,2048,128]{2,1,0:T(8,128)(2,1)}, u32[]{:S(2)}) copy-start(bf16[1,2048,128]{2,1,0:T(8,128)(2,1)} %param.39) | copy-start | bytes 1572868
  174.4 75.9 %all-to-all-start.1 = ((bf16[8,16,2048]{2,1,0:T(8,128)(2,1)}), bf16[8,16,2048]{2,1,0:T(8,128)(2,1)S(1)}, u32[]{:S(2)}, u32[]{:S(2)}) async-start(bf16[8,16,2048]{2,1,0:T(8,128)(2,1)} %bitcast.13), calls=%async_computation.2 | async-start | bytes 1048576 | tf_op jit(solution)/shard_map/all_to_all | solution.py:159
  179.9 108.9 %copy-start.12 = (bf16[2048]{0:T(1024)(128)(2,1)S(1)}, bf16[2048]{0:T(1024)(128)(2,1)}, u32[]{:S(2)}) copy-start(bf16[2048]{0:T(1024)(128)(2,1)} %param.45) | copy-start | bytes 12292
  179.9 108.9 %copy-start.10 = (f32[16,4]{0,1:T(4,128)S(1)}, f32[16,4]{0,1:T(4,128)}, u32[]{:S(2)}) copy-start(f32[16,4]{0,1:T(4,128)} %param.38) | copy-start | bytes 772
  179.9 122.7 %copy-start.4 = (bf16[16,2048]{1,0:T(8,128)(2,1)S(1)}, bf16[16,2048]{1,0:T(8,128)(2,1)}, u32[]{:S(2)}) copy-start(bf16[16,2048]{1,0:T(8,128)(2,1)} %all-reduce.4.cloned.1.call-done) | copy-start | bytes 196612
  179.9 103.3 %all-reduce.6.cloned.1.call-start = ((), (), s32[]{:S(2)}) async-start(), calls=%async_computation.7 | async-start | bytes 1179648 | tf_op jit(solution)/shard_map/psum | solution.py:169
  283.3 19.1 %all-to-all-start.2 = ((bf16[8,16,2048]{2,1,0:T(8,128)(2,1)}), bf16[8,16,2048]{2,1,0:T(8,128)(2,1)S(1)}, u32[]{:S(2)}, u32[]{:S(2)}) async-start(bf16[8,16,2048]{2,1,0:T(8,128)(2,1)} %get-tuple-element.2), calls=%async_computation.3 | async-start | bytes 1048576 | tf_op jit(solution)/shard_map/all_to_all | solution.py:170
Sparse Core Ops, SparseCore 0:
  26.4 60.8 reduce-scatter.1
  89.3 49.3 all-gather.1
  141.6 29.7 all-reduce.3
  253.1 30.1 all-reduce.5
where the time goes:
time: 312 us; the launch traced here: 311 us
  waiting for transfers between devices  137 us (44%)
  blocking collectives  115 us (37%)
  matrix products  21.6 us (7%)
  between operations  14.2 us (5%)
  starting transfers between devices  11.2 us (4%)
  other arithmetic  9.3 us (3%)
    all_gather x1, blocking collectives, per_device(): lax.all_gather(shared_up, 'ep', axis=0, tiled=True)  37.8 us
    all_gather x1, waiting for transfers between devices, per_device(): lax.all_gather(output_weight, 'ep', axis=1, tiled=True)  36.7 us
    all_gather x1, blocking collectives, per_device(): lax.all_gather(shared_gate, 'ep', axis=0, tiled=True)  31.9 us
    all_gather x1, blocking collectives, per_device(): lax.all_gather(shared_down, 'ep', axis=1, tiled=True)  31.3 us
    psum x1, waiting for transfers between devices, per_device(): summed = lax.psum(partial_rows.astype(jnp.bfloat16), 'tp')  30.3 us
    psum x1, waiting for transfers between devices, per_device(): mixed = lax.psum(partial_mix.astype(jnp.bfloat16), 'tp').astype(jnp.float32)  29.9 us
    reduce_scatter x1, waiting for transfers between devices, per_device(): lax.psum_scatter(jnp.dot(token_block, stacked, preferred_element_type=jnp...  25.8 us
    all_to_all x1, blocking collectives, per_device(): lax.all_to_all(normed, 'ep', split_axis=1, concat_axis=0, tiled=True)  14 us
  transfers between devices with their start and end apart: 6, of which 5 were waited for; matrix products, arithmetic and copies ran while one was open for 5% of the time, Pallas kernels for 0%

commit v1 on v0

--- a/solution.py
+++ b/solution.py
@@ -111,7 +111,9 @@
         preferred_element_type=jnp.float32,
     )
     partial_mix = partial_mix.astype(jnp.bfloat16).astype(jnp.float32)
-    mixed = lax.psum(partial_mix.astype(jnp.bfloat16), "tp").astype(jnp.float32)
+    mixed = jnp.sum(lax.all_gather(partial_mix.astype(jnp.bfloat16), "tp"), axis=0).astype(
+        jnp.float32
+    )
     residual = (tokens.astype(jnp.float32) + mixed).astype(jnp.bfloat16)
     ffn_in = rms_scale(residual, ffn_gain).astype(jnp.bfloat16)
     token_block = ffn_in

time: 312 us -> 285 us (0.913)
  waiting for transfers between devices: 137 us -> 108 us
  blocking collectives: 115 us -> 122 us
    psum x1 -> x0, waiting for transfers between devices: 29.9 us -> none  [per_device(): mixed = lax.psum(partial_mix.astype(jnp.bfloat16), 'tp').astype(jnp.float32)]
    all_gather x0 -> x1, blocking collectives: none -> 5.77 us  [per_device(): lax.all_gather(partial_mix.astype(jnp.bfloat16), 'tp')]
  transfers between devices with their start and end apart: 6 -> 5, of which waited for: 5 -> 4; matrix products, arithmetic and copies ran while one was open for 5% -> 6% of each run, Pallas kernels for 0% -> 0%
where the time goes in v1:
time: 285 us; the launch traced here: 284 us
  blocking collectives  122 us (43%)
  waiting for transfers between devices  108 us (38%)
  matrix products  21 us (7%)
  between operations  14.2 us (5%)
  starting transfers between devices  9.13 us (3%)
  other arithmetic  7.68 us (3%)
    all_gather x1, blocking collectives, per_device(): lax.all_gather(shared_up, 'ep', axis=0, tiled=True)  38.9 us
    all_gather x1, waiting for transfers between devices, per_device(): lax.all_gather(output_weight, 'ep', axis=1, tiled=True)  36.7 us
    all_gather x1, blocking collectives, per_device(): lax.all_gather(shared_gate, 'ep', axis=0, tiled=True)  31.7 us
    all_gather x1, blocking collectives, per_device(): lax.all_gather(shared_down, 'ep', axis=1, tiled=True)  31.4 us
    psum x1, waiting for transfers between devices, per_device(): summed = lax.psum(partial_rows.astype(jnp.bfloat16), 'tp')  31.3 us
    reduce_scatter x1, waiting for transfers between devices, per_device(): lax.psum_scatter(jnp.dot(token_block, stacked, preferred_element_type=jnp...  25.8 us
    all_to_all x1, blocking collectives, per_device(): lax.all_to_all(normed, 'ep', split_axis=1, concat_axis=0, tiled=True)  14 us
    all_to_all x1, waiting for transfers between devices, per_device(): lax.all_to_all(summed.reshape(received.shape), 'ep', split_axis=0, concat...  13.4 us
  transfers between devices with their start and end apart: 5, of which 4 were waited for; matrix products, arithmetic and copies ran while one was open for 6% of the time, Pallas kernels for 0%

profile of v1, /device:TPU:0, one launch (start us, length us, event | category | flops | bytes accessed | tf_op | source)
XLA Modules:
  0.0 284.5 jit_solution(1318093337728636448)
XLA Ops:
  7.3 0.8 convert_element_type.99
  8.0 1.0 fusion.27
  9.0 0.9 fusion.29
  10.0 14.0 %all_to_all.29 = bf16[16,8,256]{2,0,1:T(8,128)(2,1)S(1)} all-to-all(bf16[16,8,256]{2,0,1:T(8,128)(2,1)S(1)} %bitcast.84), channel_id=1, replica_groups=mesh['ep'=8,'tp'=4] {'ep'}, dimensions={1} | all-to-all | bytes 131072 | tf_op jit(solution)/shard_map/all_to_all | solution.py:54
  24.0 2.3 fusion.14
  26.3 0.7 all-gather.3.cloned.1.call-update
  27.0 0.9 fusion.70
  28.0 0.9 fusion.9
  29.3 0.1 fusion.6
  29.7 31.7 %all_gather.21 = bf16[2048,128]{1,0:T(8,128)(2,1)S(1)} all-gather(bf16[256,128]{1,0:T(8,128)(2,1)S(1)} %copy-done.5), channel_id=1, replica_groups=mesh['ep'=8,'tp'=4] {'ep'}, dimensions={0}, use_global_device_ids=true | all-gather | bytes 589824 | tf_op jit(solution)/shard_map/all_gather | solution.py:122
  61.4 25.8 %reduce-scatter.2.cloned.1.call-done = f32[16,1536]{1,0:T(8,128)} async-done(((f32[128,1536]{1,0:T(8,128)}), f32[16,1536]{1,0:T(8,128)}) %reduce-scatter.2.cloned.1.call-update) | async-done | bytes 98320 | tf_op jit(solution)/shard_map/reduce_scatter | solution.py:57
  87.3 0.9 convert.8
  88.7 5.8 %fusion = f32[16,4,1,128]{3,2,1,0:T(1,128)S(1)} fusion(f32[16,4,128,1]{2,3,1,0:T(1,128)S(1)} %bitcast.79, f32[16,4,128,128]{3,2,1,0:T(8,128)} %param.34, f32[16,4]{1,0:T(8,128)S(1)} %copy.43), kind=kOutput, calls=%fused_computation.1 | convolution fusion | flops 13631488 | bytes 4260096 | tf_op jit(solution)/shard_map/shde,shd->she/dot_general | solution.py:98
  94.7 1.5 multiply_add_fusion
  96.2 2.0 copy-done.2
  98.2 3.6 %fusion.79 = f32[16,4,1,128]{3,2,1,0:T(1,128)S(1)} fusion(f32[16,4,128,128]{3,2,1,0:T(8,128)S(1)} %multiply_add_fusion, f32[16,4,128,1]{2,3,1,0:T(1,128)S(1)} %bitcast.86), kind=kOutput, calls=%fused_computation.121 | convolution fusion | flops 12582912 | bytes 4259840 | tf_op jit(solution)/shard_map/shde,shd->she/dot_general | solution.py:101
  102.0 36.7 %all-gather.3.cloned.1.call-done = bf16[512,2048]{1,0:T(8,128)(2,1)} async-done(((bf16[512,256]{1,0:T(8,128)(2,1)}), bf16[512,2048]{1,0:T(8,128)(2,1)}) %all-gather.3.cloned.1.call-update) | async-done | bytes 2097168 | tf_op jit(solution)/shard_map/all_gather | solution.py:110
  138.7 2.0 convolution_convert_fusion.3
  140.7 5.8 %all-gather = bf16[64,2048]{1,0:T(8,128)(2,1)S(1)} all-gather(bf16[16,2048]{1,0:T(8,128)(2,1)S(1)} %convolution_convert_fusion.3), channel_id=2, replica_groups=mesh['ep'=8,'tp'=4] {'tp'}, dimensions={0}, use_global_device_ids=true | all-gather | bytes 327680 | tf_op jit(solution)/shard_map/all_gather | solution.py:114
  146.8 1.1 convolution_convert_fusion.1
  147.9 3.5 %all-to-all-start.1 = ((bf16[8,16,2048]{2,1,0:T(8,128)(2,1)}), bf16[8,16,2048]{2,1,0:T(8,128)(2,1)S(1)}, u32[]{:S(2)}, u32[]{:S(2)}) async-start(bf16[8,16,2048]{2,1,0:T(8,128)(2,1)} %bitcast.14), calls=%async_computation.2 | async-start | bytes 1048576 | tf_op jit(solution)/shard_map/all_to_all | solution.py:161
  151.5 38.9 %all_gather.22 = bf16[2048,128]{1,0:T(8,128)(2,1)S(1)} all-gather(bf16[256,128]{1,0:T(8,128)(2,1)S(1)} %copy-done.6), channel_id=1, replica_groups=mesh['ep'=8,'tp'=4] {'ep'}, dimensions={0}, use_global_device_ids=true | all-gather | bytes 589824 | tf_op jit(solution)/shard_map/all_gather | solution.py:127
  190.4 31.4 %all_gather.23 = bf16[128,2048]{1,0:T(8,128)(2,1)S(1)} all-gather(bf16[128,256]{1,0:T(8,128)(2,1)S(1)} %copy-done.7), channel_id=1, replica_groups=mesh['ep'=8,'tp'=4] {'ep'}, dimensions={1}, use_global_device_ids=true | all-gather | bytes 589824 | tf_op jit(solution)/shard_map/all_gather | solution.py:133
  221.8 0.2 fusion.80
  222.0 1.0 convolution_convert_fusion.2
  223.0 0.3 fusion.25
  223.3 2.4 convolution_convert_fusion
  225.7 31.3 %all-reduce.3.cloned.1.call-done = (bf16[8,16,2048]{2,1,0:T(8,128)(2,1)}, bf16[16,2048]{1,0:T(8,128)(2,1)}) async-done(((bf16[8,16,2048]{2,1,0:T(8,128)(2,1)}, bf16[16,2048]{1,0:T(8,128)(2,1)}), (bf16[8,16,2048]{2,1,0:T(8,128)(2,1)}, bf16[16,2048]{1,0:T(8,128)(2,1)})) %all-reduce.3.cloned.1.call-update) | async-done | bytes 589840 | tf_op jit(solution)/shard_map/psum | solution.py:171
  257.0 5.5 %all-to-all-start.2 = ((bf16[8,16,2048]{2,1,0:T(8,128)(2,1)}), bf16[8,16,2048]{2,1,0:T(8,128)(2,1)S(1)}, u32[]{:S(2)}, u32[]{:S(2)}) async-start(bf16[8,16,2048]{2,1,0:T(8,128)(2,1)} %get-tuple-element.2), calls=%async_computation.3 | async-start | bytes 1048576 | tf_op jit(solution)/shard_map/all_to_all | solution.py:172
  262.7 13.4 %all-to-all-done.2 = bf16[8,16,2048]{2,1,0:T(8,128)(2,1)S(1)} async-done(((bf16[8,16,2048]{2,1,0:T(8,128)(2,1)}), bf16[8,16,2048]{2,1,0:T(8,128)(2,1)S(1)}, u32[]{:S(2)}, u32[]{:S(2)}) %all-to-all-start.2) | async-done | bytes 524320 | tf_op jit(solution)/shard_map/all_to_all | solution.py:172
  276.1 0.3 fusion.3
  276.4 1.6 fusion.35
  (75 shorter events, 2.1 us)
Async XLA Ops:
  7.2 216.1 %copy-start = (bf16[1,128,2048]{2,1,0:T(8,128)(2,1)S(1)}, bf16[1,128,2048]{2,1,0:T(8,128)(2,1)}, u32[]{:S(2)}) copy-start(bf16[1,128,2048]{2,1,0:T(8,128)(2,1)} %param.41) | copy-start | bytes 1572868
  7.2 19.8 %copy-start.12 = (f32[4]{0:T(128)S(1)}, f32[4]{0:T(128)}, u32[]{:S(2)}) copy-start(f32[4]{0:T(128)} %param.31) | copy-start | bytes 52
  7.2 19.8 %copy-start.13 = (f32[4]{0:T(128)S(1)}, f32[4]{0:T(128)}, u32[]{:S(2)}) copy-start(f32[4]{0:T(128)} %param.32) | copy-start | bytes 52
  7.2 21.8 %copy-start.14 = (bf16[128]{0:T(256)(128)(2,1)S(1)}, bf16[128]{0:T(256)(128)(2,1)}, u32[]{:S(2)}) copy-start(bf16[128]{0:T(256)(128)(2,1)} %param.33) | copy-start | bytes 772
  7.2 21.8 %copy-start.10 = (bf16[2048]{0:T(1024)(128)(2,1)S(1)}, bf16[2048]{0:T(1024)(128)(2,1)}, u32[]{:S(2)}) copy-start(bf16[2048]{0:T(1024)(128)(2,1)} %param.36) | copy-start | bytes 12292
  7.2 21.9 %copy-start.8 = (s32[16,4]{0,1:T(4,128)S(1)}, s32[16,4]{0,1:T(4,128)}, u32[]{:S(2)}) copy-start(s32[16,4]{0,1:T(4,128)} %param.37) | copy-start | bytes 772
  7.2 22.5 %copy-start.5 = (bf16[256,128]{1,0:T(8,128)(2,1)S(1)}, bf16[256,128]{1,0:T(8,128)(2,1)}, u32[]{:S(2)}) copy-start(bf16[256,128]{1,0:T(8,128)(2,1)} %param.42) | copy-start | bytes 196612
  7.2 80.0 %reduce-scatter.2.cloned.1.call-start = ((), (), s32[]{:S(2)}) async-start(), calls=%async_computation.4 | async-start | bytes 884736 | tf_op jit(solution)/shard_map/reduce_scatter | solution.py:57
  26.3 112.5 %all-gather.3.cloned.1.call-start = ((), (), s32[]{:S(2)}) async-start(), calls=%async_computation.5 | async-start | bytes 2359296 | tf_op jit(solution)/shard_map/all_gather | solution.py:110
  88.3 6.3 %copy-start.1 = (f32[16,4,128,128]{3,2,1,0:T(8,128)S(1)}, f32[16,4,128,128]{3,2,1,0:T(8,128)}, u32[]{:S(2)}) copy-start(f32[16,4,128,128]{3,2,1,0:T(8,128)} %param.34) | copy-start | bytes 12582916
  96.2 2.0 copy-start.2
  96.2 50.3 %copy-start.3 = (bf16[16,2048]{1,0:T(8,128)(2,1)S(1)}, bf16[16,2048]{1,0:T(8,128)(2,1)}, u32[]{:S(2)}) copy-start(bf16[16,2048]{1,0:T(8,128)(2,1)} %param.23) | copy-start | bytes 196612
  98.2 53.3 %copy-start.6 = (bf16[256,128]{1,0:T(8,128)(2,1)S(1)}, bf16[256,128]{1,0:T(8,128)(2,1)}, u32[]{:S(2)}) copy-start(bf16[256,128]{1,0:T(8,128)(2,1)} %param.43) | copy-start | bytes 196612
  98.2 92.2 %copy-start.7 = (bf16[128,256]{1,0:T(8,128)(2,1)S(1)}, bf16[128,256]{1,0:T(8,128)(2,1)}, u32[]{:S(2)}) copy-start(bf16[128,256]{1,0:T(8,128)(2,1)} %param.44) | copy-start | bytes 196612
  101.8 121.1 %copy-start.4 = (bf16[1,2048,128]{2,1,0:T(8,128)(2,1)S(1)}, bf16[1,2048,128]{2,1,0:T(8,128)(2,1)}, u32[]{:S(2)}) copy-start(bf16[1,2048,128]{2,1,0:T(8,128)(2,1)} %param.39) | copy-start | bytes 1572868
  147.9 75.1 %all-to-all-start.1 = ((bf16[8,16,2048]{2,1,0:T(8,128)(2,1)}), bf16[8,16,2048]{2,1,0:T(8,128)(2,1)S(1)}, u32[]{:S(2)}, u32[]{:S(2)}) async-start(bf16[8,16,2048]{2,1,0:T(8,128)(2,1)} %bitcast.14), calls=%async_computation.2 | async-start | bytes 1048576 | tf_op jit(solution)/shard_map/all_to_all | solution.py:161
  151.4 111.2 %copy-start.11 = (bf16[2048]{0:T(1024)(128)(2,1)S(1)}, bf16[2048]{0:T(1024)(128)(2,1)}, u32[]{:S(2)}) copy-start(bf16[2048]{0:T(1024)(128)(2,1)} %param.45) | copy-start | bytes 12292
  151.4 111.2 %copy-start.9 = (f32[16,4]{0,1:T(4,128)S(1)}, f32[16,4]{0,1:T(4,128)}, u32[]{:S(2)}) copy-start(f32[16,4]{0,1:T(4,128)} %param.38) | copy-start | bytes 772
  151.4 105.6 %all-reduce.3.cloned.1.call-start = ((), (), s32[]{:S(2)}) async-start(), calls=%async_computation.6 | async-start | bytes 1179648 | tf_op jit(solution)/shard_map/psum | solution.py:171
  257.0 19.1 %all-to-all-start.2 = ((bf16[8,16,2048]{2,1,0:T(8,128)(2,1)}), bf16[8,16,2048]{2,1,0:T(8,128)(2,1)S(1)}, u32[]{:S(2)}, u32[]{:S(2)}) async-start(bf16[8,16,2048]{2,1,0:T(8,128)(2,1)} %get-tuple-element.2), calls=%async_computation.3 | async-start | bytes 1048576 | tf_op jit(solution)/shard_map/all_to_all | solution.py:172
Sparse Core Ops, SparseCore 0:
  26.4 60.8 reduce-scatter.1
  89.3 49.3 all-gather.2
  225.8 31.1 all-reduce.2
